TPU v7x, 512 devices: a whole 4x8x8 slice. The times are simulated.
512 devices in a mesh: ep: 32 (over z, x), tp: 16 (over y, core).
Axes of the slice: x: 4, y: 8, z: 8, core: 2. Of those that a mesh axis runs over, the one named last changes fastest.
Arguments:
- tokens: bfloat16 [256, 4096], P('ep', 'tp'), may hold values from -6 to 6
- norm_gain: float32 [4096], replicated, may hold values from 0.1 to 1.9
- route_experts: int32 [256, 2], P('ep'), may hold values from 0 to 63, all different within a row; in each aligned block of 8 rows (0 to 7, 8 to 15, ...) at most 2 rows name the same one
- route_logits: float32 [256, 2], P('ep'), may hold values from -4 to 4
- expert_gate: bfloat16 [64, 4096, 1024], P('ep', None, 'tp'), may hold values from -0.09375 to 0.09375
- expert_up: bfloat16 [64, 4096, 1024], P('ep', None, 'tp'), may hold values from -0.09375 to 0.09375
- expert_down: bfloat16 [64, 1024, 4096], P('ep', 'tp'), may hold values from -0.1875 to 0.1875
- dense_gate: bfloat16 [4096, 1024], P(None, 'tp'), may hold values from -0.09375 to 0.09375
- dense_up: bfloat16 [4096, 1024], P(None, 'tp'), may hold values from -0.09375 to 0.09375
- dense_down: bfloat16 [1024, 4096], P('tp'), may hold values from -0.1875 to 0.1875
- mix_weight: float32 [4096], replicated, may hold values from -0.09375 to 0.09375
- out_gain: float32 [4096], P('tp'), may hold values from 0.1 to 1.9
Outputs:
- result: bfloat16 [256, 4096], P('ep', 'tp')
Inputs may be any that keep to these rules, and one draw needn't show every extreme that they name: `route_experts`: each row names 2 different experts; the 8 rows of one index of ep (aligned blocks) name any one expert at most 2 times, and some block names some expert exactly 2 times; every expert is named somewhere.
All inputs are finite; a program needn't handle non-finite values.
Results may differ from a plain program's by a relative error of at most 0.0025.
Values may be sent and summed in bfloat16 or wider, within the bound.
A program may use at most 64 MiB of HBM per device.

v0:
```python
import jax
import jax.numpy as jnp
from jax import lax
from jax.sharding import Mesh
from jax.sharding import PartitionSpec as P

CAP = 2
TP = ("tp_0", "tp_1")
norm_eps = 1e-06


def summed_rows(x, axes, dim):
    if not axes:
        return x
    nearer = lax.psum_scatter(x, axes[0], scatter_dimension=dim, tiled=True)
    return summed_rows(nearer, axes[1:], dim)


def local(
    tokens,
    norm_gain,
    route_experts,
    route_logits,
    expert_gate,
    expert_up,
    expert_down,
    dense_gate,
    dense_up,
    dense_down,
    mix_weight,
    out_gain,
):
    tok_rows, width_part = tokens.shape
    groups = lax.axis_size(TP)
    width = width_part * groups
    whole_rows = lax.all_gather(tokens, TP, axis=1, tiled=True).astype(jnp.float32)
    normed = (
        whole_rows
        * lax.rsqrt(jnp.mean(whole_rows * whole_rows, axis=1, keepdims=True) + norm_eps)
        * norm_gain
    ).astype(jnp.bfloat16)
    weights = jax.nn.softmax(route_logits, axis=-1)
    top_count = route_experts.shape[1]
    local_experts = expert_gate.shape[0]
    peer_count = lax.axis_size("ep")
    experts = local_experts * peer_count
    dense_hidden = (
        jax.nn.silu(jnp.dot(normed, dense_gate, preferred_element_type=jnp.float32))
        * jnp.dot(normed, dense_up, preferred_element_type=jnp.float32)
    ).astype(jnp.bfloat16)
    dense_out = summed_rows(
        jnp.dot(dense_hidden, dense_down, preferred_element_type=jnp.float32), TP, 1
    )
    mix_gate = jax.nn.sigmoid(
        jnp.dot(normed.astype(jnp.float32), mix_weight, precision=lax.Precision.HIGHEST)
    )
    flat_routes = route_experts.reshape(-1)
    expert_ids = jnp.arange(experts, dtype=jnp.int32)
    capacity = CAP
    slot_count = experts * capacity
    route_hits = (flat_routes[:, None] == expert_ids[None, :]).astype(jnp.int32)
    before = jnp.cumsum(route_hits, axis=0) - route_hits
    slot_rank = jnp.sum(before * route_hits, axis=1)
    position = flat_routes * capacity + slot_rank
    onehot_place = (position[:, None] == jnp.arange(slot_count, dtype=jnp.int32)[None, :]).astype(
        jnp.float32
    )
    placing = jnp.sum(onehot_place.reshape(tok_rows, top_count, slot_count), axis=1).T.astype(
        jnp.bfloat16
    )
    outgoing = jnp.dot(placing, normed, preferred_element_type=jnp.float32).astype(jnp.bfloat16)
    received = lax.all_to_all(outgoing, "ep", split_axis=0, concat_axis=0, tiled=True)
    arranged = (
        received.reshape(peer_count, local_experts, capacity, width)
        .transpose(1, 0, 2, 3)
        .reshape(local_experts, peer_count * capacity, width)
    )
    gate_act = jnp.einsum("erd,edf->erf", arranged, expert_gate, preferred_element_type=jnp.float32)
    up_act = jnp.einsum("erd,edf->erf", arranged, expert_up, preferred_element_type=jnp.float32)
    hidden = (jax.nn.silu(gate_act) * up_act).astype(jnp.bfloat16)
    partial_value = jnp.einsum(
        "erf,efd->erd", hidden, expert_down, preferred_element_type=jnp.float32
    )
    summed = lax.psum_scatter(partial_value, TP, scatter_dimension=2, tiled=True)
    back_send = (
        summed.reshape(local_experts, peer_count, capacity, width_part)
        .transpose(1, 0, 2, 3)
        .reshape(slot_count, width_part)
    )
    returned = lax.all_to_all(back_send, "ep", split_axis=0, concat_axis=0, tiled=True)
    combine_map = jnp.sum(
        (onehot_place * weights.reshape(-1)[:, None]).reshape(tok_rows, top_count, slot_count),
        axis=1,
    )
    expert_mix = jnp.dot(combine_map, returned, precision=lax.Precision.HIGHEST)
    combined = expert_mix + mix_gate[:, None] * dense_out
    squares_out = lax.psum(jnp.sum(combined * combined, axis=1), TP)
    result = combined * lax.rsqrt(squares_out[:, None] / width + norm_eps) * out_gain
    return result.astype(jnp.bfloat16)


def solution(mesh):
    split = Mesh(mesh.devices.reshape(mesh.shape["ep"], 8, 2), ("ep", "tp_0", "tp_1"))
    in_specs = (
        P("ep", TP),
        P(),
        P("ep", None),
        P("ep", None),
        P("ep", None, TP),
        P("ep", None, TP),
        P("ep", TP, None),
        P(None, TP),
        P(None, TP),
        P(TP, None),
        P(),
        P(TP),
    )
    out_specs = P("ep", TP)
    return jax.shard_map(local, mesh=split, in_specs=in_specs, out_specs=out_specs, check_vma=False)
```

profile of v0, /device:TPU:2, one launch (start us, length us, event | category | flops | bytes accessed | tf_op | source)
XLA Modules:
  0.0 229.2 jit_solution(5264460515615627035)
XLA Ops:
  6.5 0.0 copy-start
  6.5 0.0 reduce-scatter.4.cloned.1.call-start
  6.5 0.8 reduce_max.9
  7.3 0.7 fusion.26
  8.0 0.7 fusion.25
  8.7 0.8 copy.34
  9.5 0.1 eq.30
  9.6 0.1 fusion.17
  9.7 0.2 select_reduce_fusion.1
  9.8 0.1 reduce_sum.57
  9.9 0.1 copy.36
  10.0 18.0 %all_gather.3 = bf16[8,4096]{1,0:T(8,128)(2,1)S(1)} all-gather(bf16[8,256]{1,0:T(8,128)(2,1)} %param.12), channel_id=1, replica_groups=mesh['ep'=32,'tp_0'=8,'tp_1'=2] {'tp_0','tp_1'}, dimensions={1}, use_global_device_ids=true | all-gather | bytes 69632 | tf_op jit(solution)/shard_map/all_gather | solution.py:36
  28.0 0.1 fusion.8
  28.2 0.1 convert_reduce_fusion
  28.2 1.2 convolution_convert_fusion
  29.5 0.4 all_to_all.14
  29.9 41.8 %all_to_all.21 = bf16[32,4,4096]{2,1,0:T(4,128)(2,1)S(1)} all-to-all(bf16[32,4,4096]{2,1,0:T(4,128)(2,1)S(1)} %all_to_all.14), channel_id=1, replica_groups=mesh['ep'=32,'tp_0'=8,'tp_1'=2] {'ep'}, dimensions={0} | all-to-all | bytes 2097152 | tf_op jit(solution)/shard_map/all_to_all | solution.py:72
  71.7 0.5 reshape.67
  72.3 2.0 copy.41
  74.3 1.6 reshape.68
  75.9 0.0 copy-done.1
  75.9 0.4 fusion.35
  76.3 0.0 copy-done
  76.3 3.4 %fusion.1 = f32[2,64,4096]{2,1,0:T(8,128)} fusion(bf16[2,64,4096]{2,1,0:T(8,128)(2,1)S(1)} %copy-done, bf16[2,64,4096]{2,1,0:T(8,128)(2,1)S(1)} %reshape.68, bf16[2,4096,64]{1,2,0:T(8,128)(2,1)} %param.17, f32[2,64,64]{2,1,0:T(8,128)S(1)} %fusion.35), kind=kOutput, calls=%fused_computation.3 | convolution fusion | flops 134266880 | bytes 5275648 | tf_op jit(solution)/shard_map/erf,efd->erd/dot_general | solution.py:81
  79.7 0.0 copy-start.7
  79.7 0.0 reduce-scatter.4.cloned.1.call-update
  79.7 0.0 copy-start.6
  79.8 0.0 reduce-scatter.6.cloned.1.call-start
  79.8 0.9 copy-done.2
  80.7 0.3 fusion.31
  81.0 0.0 copy-done.4
  81.1 1.3 fusion.3
  82.3 0.0 reduce-scatter.6.cloned.1.call-update
  82.4 53.8 %reduce-scatter.4.cloned.1.call-done = f32[2,64,256]{2,1,0:T(8,128)} async-done(((f32[2,64,4096]{2,1,0:T(8,128)}), f32[2,64,256]{2,1,0:T(8,128)}) %reduce-scatter.4.cloned.1.call-update) | async-done | bytes 131088 | tf_op jit(solution)/shard_map/reduce_scatter | solution.py:84
  136.1 1.0 reshape.69
  137.1 0.7 copy.39
  137.8 10.5 %all-to-all-start.1 = ((f32[32,4,256]{2,1,0:T(4,128)}), f32[32,4,256]{2,1,0:T(4,128)S(1)}, u32[]{:S(2)}, u32[]{:S(2)}) async-start(f32[32,4,256]{2,1,0:T(4,128)} %copy.39), calls=%async_computation.2 | async-start | bytes 262144 | tf_op jit(solution)/shard_map/all_to_all | solution.py:90
  148.3 0.0 reduce-scatter.8.cloned.1.call-start
  148.4 28.9 %reduce-scatter.6.cloned.1.call-done = f32[8,512]{1,0:T(8,128)} async-done(((f32[8,4096]{1,0:T(8,128)}), f32[8,512]{1,0:T(8,128)}) %reduce-scatter.6.cloned.1.call-update) | async-done | bytes 16400 | tf_op jit(solution)/shard_map/reduce_scatter | solution.py:15
  177.3 0.0 reduce-scatter.8.cloned.1.call-update
  177.3 0.3 fusion.7
  177.6 0.0 all-to-all-done.1
  177.7 0.1 all_to_all.18
  177.7 16.9 %reduce-scatter.8.cloned.1.call-done = f32[8,256]{1,0:T(8,128)} async-done(((f32[8,512]{1,0:T(8,128)}), f32[8,256]{1,0:T(8,128)}) %reduce-scatter.8.cloned.1.call-update) | async-done | bytes 8208 | tf_op jit(solution)/shard_map/reduce_scatter | solution.py:15
  194.6 1.0 multiply_reduce_fusion
  195.6 26.3 %psum.7 = f32[8]{0:T(128)S(1)} all-reduce(f32[8]{0:T(128)S(1)} %get-tuple-element.7), channel_id=1, replica_groups=mesh['ep'=32,'tp_0'=8,'tp_1'=2] {'tp_0','tp_1'}, use_global_device_ids=true, to_apply=%region_11.12 | all-reduce | flops 8 | bytes 64 | tf_op jit(solution)/shard_map/psum | solution.py:97
  222.0 0.0 copy-done.6
  222.0 0.7 multiply_convert_fusion
  (13 shorter events, 0.1 us)
Async XLA Ops:
  6.5 69.8 %copy-start = (bf16[2,64,4096]{2,1,0:T(8,128)(2,1)S(1)}, bf16[2,64,4096]{2,1,0:T(8,128)(2,1)}, u32[]{:S(2)}) copy-start(bf16[2,64,4096]{2,1,0:T(8,128)(2,1)} %param.18) | copy-start | bytes 3145732
  6.5 129.6 %reduce-scatter.4.cloned.1.call-start = ((), (), s32[]{:S(2)}) async-start(), calls=%async_computation.5 | async-start | bytes 2228224 | tf_op jit(solution)/shard_map/reduce_scatter | solution.py:84
  74.3 1.6 copy-start.1
  79.7 1.0 copy-start.2
  79.7 1.0 copy-start.5
  79.7 1.3 copy-start.3
  79.7 1.4 copy-start.4
  79.7 97.6 %copy-start.7 = (f32[4096]{0:T(1024)S(1)}, f32[4096]{0:T(1024)}, u32[]{:S(2)}) copy-start(f32[4096]{0:T(1024)} %param.22) | copy-start | bytes 49156
  79.7 142.2 %copy-start.6 = (f32[256]{0:T(256)S(1)}, f32[256]{0:T(256)}, u32[]{:S(2)}) copy-start(f32[256]{0:T(256)} %param.23) | copy-start | bytes 3076
  79.8 97.6 %reduce-scatter.6.cloned.1.call-start = ((), (), s32[]{:S(2)}) async-start(), calls=%async_computation.6 | async-start | bytes 147456 | tf_op jit(solution)/shard_map/reduce_scatter | solution.py:15
  137.8 39.8 %all-to-all-start.1 = ((f32[32,4,256]{2,1,0:T(4,128)}), f32[32,4,256]{2,1,0:T(4,128)S(1)}, u32[]{:S(2)}, u32[]{:S(2)}) async-start(f32[32,4,256]{2,1,0:T(4,128)} %copy.39), calls=%async_computation.2 | async-start | bytes 262144 | tf_op jit(solution)/shard_map/all_to_all | solution.py:90
  148.3 46.3 %reduce-scatter.8.cloned.1.call-start = ((), (), s32[]{:S(2)}) async-start(), calls=%async_computation.7 | async-start | bytes 24576 | tf_op jit(solution)/shard_map/reduce_scatter | solution.py:15
Sparse Core Ops, SparseCore 0:
  79.9 56.2 reduce-scatter.3
  138.9 38.3 reduce-scatter.5
  180.0 14.5 reduce-scatter.7
where the time goes:
time: 230 us; the launch traced here: 229 us
  waiting for transfers between devices  99.7 us (43%)
  blocking collectives  86.2 us (37%)
  between operations  13.2 us (6%)
  starting transfers between devices  10.6 us (5%)
  local copies, waits for them, and re-layouts  8.3 us (4%)
  matrix products  7.8 us (3%)
  other arithmetic  3.38 us (1%)
    reduce_scatter x1, waiting for transfers between devices, local(): lax.psum_scatter(partial_value, TP, scatter_dimension=2, tiled=True)  53.8 us
    reduce_scatter x2, waiting for transfers between devices, summed_rows(): nearer = lax.psum_scatter(x, axes[0], scatter_dimension=dim, tiled=True)  45.8 us
    all_to_all x1, blocking collectives, local(): lax.all_to_all(outgoing, 'ep', split_axis=0, concat_axis=0, tiled=True)  41.8 us
    psum x1, blocking collectives, local(): squares_out = lax.psum(jnp.sum(combined * combined, axis=1), TP)  26.3 us
    all_gather x1, blocking collectives, local(): lax.all_gather(tokens, TP, axis=1, tiled=True).astype(jnp.float32)  18 us
    all_to_all x1, starting transfers between devices, local(): lax.all_to_all(back_send, 'ep', split_axis=0, concat_axis=0, tiled=True)  10.5 us
  transfers between devices with their start and end apart: 4, of which 3 were waited for; matrix products, arithmetic and copies ran while one was open for 2% of the time, Pallas kernels for 0%

commit v1 on v0

--- a/solution.py
+++ b/solution.py
@@ -7,6 +7,13 @@
 CAP = 2
 TP = ("tp_0", "tp_1")
 norm_eps = 1e-06
+
+
+def swapped_in(array, mesh_axis, dim):
+    size = lax.axis_size(mesh_axis)
+    blocks = jnp.stack([array for _ in range(size)])
+    blocks = lax.all_to_all(blocks, mesh_axis, split_axis=0, concat_axis=0)
+    return jnp.concatenate(blocks, axis=dim)
 
 
 def summed_rows(x, axes, dim):
@@ -33,7 +40,7 @@
     tok_rows, width_part = tokens.shape
     groups = lax.axis_size(TP)
     width = width_part * groups
-    whole_rows = lax.all_gather(tokens, TP, axis=1, tiled=True).astype(jnp.float32)
+    whole_rows = swapped_in(tokens, TP, 1).astype(jnp.float32)
     normed = (
         whole_rows
         * lax.rsqrt(jnp.mean(whole_rows * whole_rows, axis=1, keepdims=True) + norm_eps)

time: 230 us -> 223 us (0.970)
  blocking collectives: 86.2 us -> 68.2 us
  starting transfers between devices: 10.6 us -> 18 us
    all_gather x1 -> x0, blocking collectives: 18 us -> none  [local(): lax.all_gather(tokens, TP, axis=1, tiled=True).astype(jnp.float32)]
    all_to_all x0 -> x1, starting transfers between devices: none -> 7.21 us  [swapped_in(): blocks = lax.all_to_all(blocks, mesh_axis, split_axis=0, concat_axis=0)]
    all_to_all x0 -> x1, waiting for transfers between devices: none -> 4.26 us  [swapped_in(): blocks = lax.all_to_all(blocks, mesh_axis, split_axis=0, concat_axis=0)]
  transfers between devices with their start and end apart: 4 -> 5, of which waited for: 3 -> 4; matrix products, arithmetic and copies ran while one was open for 2% -> 3% of each run, Pallas kernels for 0% -> 0%
where the time goes in v1:
time: 223 us
  waiting for transfers between devices  102 us (46%)
  blocking collectives  68.2 us (31%)
  starting transfers between devices  18 us (8%)
  between operations  13.3 us (6%)
  local copies, waits for them, and re-layouts  9.73 us (4%)
  matrix products  6.91 us (3%)
  other arithmetic  4.12 us (2%)
    reduce_scatter x1, waiting for transfers between devices, local(): lax.psum_scatter(partial_value, TP, scatter_dimension=2, tiled=True)  52.1 us
    reduce_scatter x2, waiting for transfers between devices, summed_rows(): nearer = lax.psum_scatter(x, axes[0], scatter_dimension=dim, tiled=True)  45.9 us
    all_to_all x1, blocking collectives, local(): lax.all_to_all(outgoing, 'ep', split_axis=0, concat_axis=0, tiled=True)  41.9 us
    psum x1, blocking collectives, local(): squares_out = lax.psum(jnp.sum(combined * combined, axis=1), TP)  26.3 us
    all_to_all x1, starting transfers between devices, local(): lax.all_to_all(back_send, 'ep', split_axis=0, concat_axis=0, tiled=True)  10.7 us
    all_to_all x1, starting transfers between devices, swapped_in(): blocks = lax.all_to_all(blocks, mesh_axis, split_axis=0, concat_axis=0)  7.21 us
  transfers between devices with their start and end apart: 5, of which 4 were waited for; matrix products, arithmetic and copies ran while one was open for 3% of the time, Pallas kernels for 0%

profile of v1, /device:TPU:2, one launch (start us, length us, event | category | flops | bytes accessed | tf_op | source)
XLA Modules:
  0.0 222.7 jit_solution(2544578256830319529)
XLA Ops:
  6.5 0.0 copy-start
  6.5 1.4 stack.2
  7.9 7.2 %all-to-all-start = ((bf16[16,8,256]{2,1,0:T(8,128)(2,1)}), bf16[16,8,256]{2,1,0:T(8,128)(2,1)S(1)}, u32[]{:S(2)}, u32[]{:S(2)}) async-start(bf16[16,8,256]{2,1,0:T(8,128)(2,1)} %stack.2), calls=%async_computation | async-start | bytes 131072 | tf_op jit(solution)/shard_map/all_to_all | solution.py:15
  15.1 0.0 reduce-scatter.4.cloned.1.call-start
  15.2 0.7 reduce_max.9
  15.9 0.7 fusion.23
  16.6 0.8 copy.34
  17.4 0.1 eq.30
  17.4 0.1 fusion.14
  17.5 0.2 select_reduce_fusion.1
  17.7 0.1 reduce_sum.57
  17.8 0.7 fusion.22
  18.5 0.1 copy.36
  18.6 0.1 convert_reduce_fusion
  18.7 4.3 %all-to-all-done = bf16[16,8,256]{2,1,0:T(8,128)(2,1)S(1)} async-done(((bf16[16,8,256]{2,1,0:T(8,128)(2,1)}), bf16[16,8,256]{2,1,0:T(8,128)(2,1)S(1)}, u32[]{:S(2)}, u32[]{:S(2)}) %all-to-all-start) | async-done | bytes 65568 | tf_op jit(solution)/shard_map/all_to_all | solution.py:15
  22.9 0.1 multiply_reduce_fusion
  23.1 0.8 multiply_convert_fusion
  23.9 0.5 convolution_convert_fusion
  24.4 0.4 all_to_all.18
  24.8 41.9 %all_to_all.26 = bf16[32,4,4096]{2,1,0:T(4,128)(2,1)S(1)} all-to-all(bf16[32,4,4096]{2,1,0:T(4,128)(2,1)S(1)} %all_to_all.18), channel_id=1, replica_groups=mesh['ep'=32,'tp_0'=8,'tp_1'=2] {'ep'}, dimensions={0} | all-to-all | bytes 2097152 | tf_op jit(solution)/shard_map/all_to_all | solution.py:79
  66.7 0.5 reshape.73
  67.3 2.0 copy.41
  69.3 1.6 reshape.74
  70.9 0.4 fusion.26
  71.3 0.0 copy-done
  71.3 3.4 %fusion.1 = f32[2,64,4096]{2,1,0:T(8,128)} fusion(bf16[2,64,4096]{2,1,0:T(8,128)(2,1)S(1)} %copy-done, bf16[2,64,4096]{2,1,0:T(8,128)(2,1)S(1)} %reshape.74, bf16[2,4096,64]{1,2,0:T(8,128)(2,1)} %param.17, f32[2,64,64]{2,1,0:T(8,128)S(1)} %fusion.26), kind=kOutput, calls=%fused_computation.3 | convolution fusion | flops 134266880 | bytes 5275648 | tf_op jit(solution)/shard_map/erf,efd->erd/dot_general | solution.py:88
  74.7 0.0 reduce-scatter.4.cloned.1.call-update
  74.7 0.0 copy-start.5
  74.7 0.0 reduce-scatter.6.cloned.1.call-start
  74.8 0.9 copy-done.2
  75.7 0.2 fusion.27
  76.0 0.1 copy-done.4
  76.0 1.2 fusion.3
  77.3 0.0 reduce-scatter.6.cloned.1.call-update
  77.3 52.1 %reduce-scatter.4.cloned.1.call-done = f32[2,64,256]{2,1,0:T(8,128)} async-done(((f32[2,64,4096]{2,1,0:T(8,128)}), f32[2,64,256]{2,1,0:T(8,128)}) %reduce-scatter.4.cloned.1.call-update) | async-done | bytes 131088 | tf_op jit(solution)/shard_map/reduce_scatter | solution.py:91
  129.4 1.0 reshape.75
  130.4 0.7 copy.39
  131.1 10.7 %all-to-all-start.2 = ((f32[32,4,256]{2,1,0:T(4,128)}), f32[32,4,256]{2,1,0:T(4,128)S(1)}, u32[]{:S(2)}, u32[]{:S(2)}) async-start(f32[32,4,256]{2,1,0:T(4,128)} %copy.39), calls=%async_computation.3 | async-start | bytes 262144 | tf_op jit(solution)/shard_map/all_to_all | solution.py:97
  141.8 0.0 reduce-scatter.8.cloned.1.call-start
  141.9 28.9 %reduce-scatter.6.cloned.1.call-done = f32[8,512]{1,0:T(8,128)} async-done(((f32[8,4096]{1,0:T(8,128)}), f32[8,512]{1,0:T(8,128)}) %reduce-scatter.6.cloned.1.call-update) | async-done | bytes 16400 | tf_op jit(solution)/shard_map/reduce_scatter | solution.py:22
  170.7 0.0 reduce-scatter.8.cloned.1.call-update
  170.8 0.2 fusion.7
  171.0 0.0 all-to-all-done.2
  171.0 0.1 all_to_all.22
  171.1 17.1 %reduce-scatter.8.cloned.1.call-done = f32[8,256]{1,0:T(8,128)} async-done(((f32[8,512]{1,0:T(8,128)}), f32[8,256]{1,0:T(8,128)}) %reduce-scatter.8.cloned.1.call-update) | async-done | bytes 8208 | tf_op jit(solution)/shard_map/reduce_scatter | solution.py:22
  188.2 1.0 multiply_reduce_fusion.1
  189.1 26.3 %psum.7 = f32[8]{0:T(128)S(1)} all-reduce(f32[8]{0:T(128)S(1)} %get-tuple-element.7), channel_id=1, replica_groups=mesh['ep'=32,'tp_0'=8,'tp_1'=2] {'tp_0','tp_1'}, use_global_device_ids=true, to_apply=%region_11.12 | all-reduce | flops 8 | bytes 64 | tf_op jit(solution)/shard_map/psum | solution.py:104
  215.5 0.7 multiply_convert_fusion.1
  (15 shorter events, 0.1 us)
Async XLA Ops:
  6.5 64.7 %copy-start = (bf16[2,64,4096]{2,1,0:T(8,128)(2,1)S(1)}, bf16[2,64,4096]{2,1,0:T(8,128)(2,1)}, u32[]{:S(2)}) copy-start(bf16[2,64,4096]{2,1,0:T(8,128)(2,1)} %param.18) | copy-start | bytes 3145732
  7.9 15.0 %all-to-all-start = ((bf16[16,8,256]{2,1,0:T(8,128)(2,1)}), bf16[16,8,256]{2,1,0:T(8,128)(2,1)S(1)}, u32[]{:S(2)}, u32[]{:S(2)}) async-start(bf16[16,8,256]{2,1,0:T(8,128)(2,1)} %stack.2), calls=%async_computation | async-start | bytes 131072 | tf_op jit(solution)/shard_map/all_to_all | solution.py:15
  15.1 114.2 %reduce-scatter.4.cloned.1.call-start = ((), (), s32[]{:S(2)}) async-start(), calls=%async_computation.6 | async-start | bytes 2228224 | tf_op jit(solution)/shard_map/reduce_scatter | solution.py:91
  69.3 1.6 copy-start.1
  74.7 1.0 copy-start.2
  74.7 1.3 copy-start.3
  74.7 1.4 copy-start.4
  74.7 96.1 %copy-start.6 = (f32[4096]{0:T(1024)S(1)}, f32[4096]{0:T(1024)}, u32[]{:S(2)}) copy-start(f32[4096]{0:T(1024)} %param.22) | copy-start | bytes 49156
  74.7 140.8 %copy-start.5 = (f32[256]{0:T(256)S(1)}, f32[256]{0:T(256)}, u32[]{:S(2)}) copy-start(f32[256]{0:T(256)} %param.23) | copy-start | bytes 3076
  74.7 96.0 %reduce-scatter.6.cloned.1.call-start = ((), (), s32[]{:S(2)}) async-start(), calls=%async_computation.7 | async-start | bytes 147456 | tf_op jit(solution)/shard_map/reduce_scatter | solution.py:22
  131.1 40.0 %all-to-all-start.2 = ((f32[32,4,256]{2,1,0:T(4,128)}), f32[32,4,256]{2,1,0:T(4,128)S(1)}, u32[]{:S(2)}, u32[]{:S(2)}) async-start(f32[32,4,256]{2,1,0:T(4,128)} %copy.39), calls=%async_computation.3 | async-start | bytes 262144 | tf_op jit(solution)/shard_map/all_to_all | solution.py:97
  141.8 46.4 %reduce-scatter.8.cloned.1.call-start = ((), (), s32[]{:S(2)}) async-start(), calls=%async_computation.8 | async-start | bytes 24576 | tf_op jit(solution)/shard_map/reduce_scatter | solution.py:22
Sparse Core Ops, SparseCore 0:
  74.8 54.4 reduce-scatter.3
  132.1 38.5 reduce-scatter.5
  173.5 14.6 reduce-scatter.7
